TPU v7x, 32 devices: a whole 2x2x4 slice. The times are simulated.
32 devices in a mesh: sp: 8 (over z, y), tp: 4 (over x, core).
Axes of the slice: x: 2, y: 2, z: 4, core: 2. Of those that a mesh axis runs over, the one named last changes fastest.
Arguments:
- queries: bfloat16 [6144, 1536], P('sp', 'tp'), may hold values from -130 to 130, as said below
- keys: bfloat16 [6144, 512], P('sp', 'tp'), may hold values from -6 to 6
- values: bfloat16 [6144, 512], P('sp', 'tp'), may hold values from -6 to 6
- residual: bfloat16 [6144, 2048], P(('sp', 'tp')), may hold values from -6 to 6
- sinks: float32 [12], P('tp'), may hold values from 2 to 6
- out_weight: bfloat16 [1536, 2048], P('tp'), may hold values from -0.15625 to 0.15625
- up_weight: bfloat16 [2048, 8192], P('sp', 'tp'), may hold values from -0.125 to 0.125
- down_weight: bfloat16 [8192, 2048], P('tp', 'sp'), may hold values from -0.0625 to 0.0625
- gains: float32 [2, 2048], replicated, may hold values from 0.1 to 1.9
- biases: float32 [2, 2048], replicated, may hold values from -3 to 3
Outputs:
- layer_out: bfloat16 [6144, 2048], P(('sp', 'tp'))
Inputs may be any that keep to these rules, and one draw needn't show every extreme that they name: `queries`: entries of order one, with some rows far larger in some draws.
All inputs are finite; a program needn't handle non-finite values.
Results may differ from a plain program's by a relative error of at most 0.0095.
Values may be sent and summed in bfloat16 or wider, within the bound.
A program may use at most 128 MiB of HBM per device.

v0:
```python
import functools

import jax
import jax.numpy as jnp
from jax import lax
from jax.experimental import pallas as pl
from jax.experimental.pallas import tpu as pltpu
from jax.sharding import PartitionSpec as P

HEADS = 12
HEAD = 128
WINDOW = 128


deep_alpha = 1.6817928
norm_eps = 1e-05
neg_big = -1e30


def from_behind(block, axis, distance):
    devices = range(lax.axis_size(axis))
    route = [(i - distance, i) for i in devices if i - distance in devices]
    return lax.ppermute(block, axis, route)


def layer_norm(stream, gain, bias):
    mean = jnp.mean(stream, axis=-1, keepdims=True)
    spread = jnp.mean(jnp.square(stream - mean), axis=-1, keepdims=True)
    return ((stream - mean) * lax.rsqrt(spread + norm_eps) * gain + bias).astype(jnp.bfloat16)


def attend(queries, keys, values, before, sinks, offset, rank_tp):
    tokens = keys.shape[0]
    kv_local = keys.shape[1] // HEAD
    heads_local = sinks.shape[0]
    group = heads_local // kv_local
    blocks = tokens // WINDOW
    q_blocks = queries.reshape(blocks, WINDOW, kv_local, group, HEAD)
    key_ext = jnp.concatenate([before[0], keys], axis=0).reshape(tokens + WINDOW, kv_local, HEAD)
    val_ext = jnp.concatenate([before[1], values], axis=0).reshape(tokens + WINDOW, kv_local, HEAD)
    key_win = jnp.concatenate(
        [
            key_ext[:tokens].reshape(blocks, WINDOW, kv_local, HEAD),
            key_ext[WINDOW:].reshape(blocks, WINDOW, kv_local, HEAD),
        ],
        axis=1,
    )
    val_win = jnp.concatenate(
        [
            val_ext[:tokens].reshape(blocks, WINDOW, kv_local, HEAD),
            val_ext[WINDOW:].reshape(blocks, WINDOW, kv_local, HEAD),
        ],
        axis=1,
    )
    logits = jnp.einsum(
        "nqkgd,nskd->nkgqs", q_blocks, key_win, preferred_element_type=jnp.float32
    ) * HEAD ** (-0.5)
    q_index = jnp.arange(WINDOW, dtype=jnp.int32)[:, None]
    k_index = jnp.arange(2 * WINDOW, dtype=jnp.int32)[None, :]
    dist = q_index + WINDOW - k_index
    block_id = jnp.arange(blocks, dtype=jnp.int32)[:, None, None]
    key_pos = offset + block_id * WINDOW - WINDOW + k_index
    valid = (dist >= 0) & (dist < WINDOW) & (key_pos >= 0)
    heads = (jnp.arange(heads_local, dtype=jnp.int32) + rank_tp * heads_local).astype(jnp.float32)
    slopes = jnp.exp2(-8.0 * (heads + 1.0) / HEADS).reshape(kv_local, group)[:, :, None, None]
    logits = logits - slopes * dist.astype(jnp.float32)
    logits = jnp.where(valid[:, None, None], logits, neg_big)
    sink = sinks.reshape(kv_local, group)[:, :, None, None]
    top = jnp.maximum(jnp.max(logits, axis=-1, keepdims=True), sink)
    probs = jnp.exp(logits - top)
    denom = jnp.sum(probs, axis=-1, keepdims=True) + jnp.exp(sink - top)
    weight = (probs / denom).astype(jnp.bfloat16)
    attended = jnp.einsum("nkgqs,nskd->nqkgd", weight, val_win, preferred_element_type=jnp.float32)
    return attended.astype(jnp.bfloat16).reshape(tokens, heads_local * HEAD)


MESH = pl.DeviceIdType.MESH
LANES = 128


def norm_rows(stream, gain, bias):
    mean = jnp.mean(stream, axis=-1, keepdims=True)
    spread = jnp.mean(jnp.square(stream - mean), axis=-1, keepdims=True)
    return (stream - mean) * lax.rsqrt(spread + norm_eps) * gain + bias


def block_kernel(
    n, m, q_ref, k_ref, v_ref, sinks_ref, slopes_ref, proj_ref, up_ref, down_ref, res_ref,
    gains_ref, biases_ref, out_ref, key_ext, val_ext, attended, mix_ref, up_all, down_all, mix_in, normed, act, terms, terms_in, total,
    tail_send, tail_recv, ring_send, ring_recv, mix_send, mix_recv, row_send, row_recv, sum_send, sum_recv,
):
    me, rank = lax.axis_index("sp"), lax.axis_index("tp")
    depth, hidden = up_ref.shape
    half = depth // 2
    own_rows, width = res_ref.shape
    step_rows = 32

    odd = lax.rem(me, 2)
    place = (1 - odd) * lax.div(me, 2) + odd * (n - 1 - lax.div(me, 2))

    def member(at):
        at = lax.rem(at + n, n)
        back = lax.div(at, n // 2)
        return (1 - back) * (2 * at) + back * (2 * (n - 1 - at) + 1)

    right, left = member(place + 1), member(place - 1)

    def peer(k):
        return lax.rem(rank + k, m)

    barrier = pltpu.get_barrier_semaphore()
    after, ahead = lax.rem(me + 1, n), lax.rem(me + n - 1, n)
    for there in (left, right, after, ahead):
        pl.semaphore_signal(barrier, inc=1, device_id=(there, rank), device_id_type=MESH)
    for k in range(1, m):
        pl.semaphore_signal(barrier, inc=1, device_id=(me, peer(k)), device_id_type=MESH)
    pl.semaphore_wait(barrier, m + 3)

    def remote(source, target, send, recv, device):
        return pltpu.make_async_remote_copy(
            src_ref=source, dst_ref=target, send_sem=send, recv_sem=recv,
            device_id=device, device_id_type=MESH,
        )

    def hop(which, s, d, c):
        owner = member(place - s) if d == 0 else member(place + s)
        if which == 0:
            rows = half // 2
            off = d * half + c * rows
            target = up_all.at[pl.ds(pl.multiple_of(owner * depth + off, rows), rows)]
            source = up_ref.at[pl.ds(off, rows)] if s == 0 else target
        else:
            rows = hidden // 2
            target = down_all.at[2 * owner + d, pl.ds(c * rows, rows)]
            source = target
            if s == 0:
                source = down_ref.at[pl.ds(c * rows, rows), pl.ds(d * half, half)]
        return remote(
            source, target, ring_send.at[which, s, d, c], ring_recv.at[which, s, d, c],
            (right if d == 0 else left, rank),
        )

    def launch(which):
        for c in range(2):
            for d in range(2):
                hop(which, 0, d, c).start()

    def serve(which, s, c):
        for d in range(2):
            hop(which, s, d, c).wait_recv()
            if s + 1 < n - 1:
                hop(which, s + 1, d, c).start()

    def serve_up(s):
        for c in range(2):
            serve(0, s, c)
        if s == max(n - 3, 0):
            launch(1)

    tokens = q_ref.shape[0]
    tails = [
        remote(
            ref.at[pl.ds(tokens - WINDOW, WINDOW)], ext.at[pl.ds(0, WINDOW)],
            tail_send.at[i], tail_recv.at[i], (after, rank),
        )
        for i, (ref, ext) in enumerate(((k_ref, key_ext), (v_ref, val_ext)))
    ]
    for copy in tails:
        copy.start()
    launch(0)
    key_ext[WINDOW:] = k_ref[...]
    val_ext[WINDOW:] = v_ref[...]
    up_all[pl.ds(pl.multiple_of(me * depth, depth), depth)] = up_ref[...]
    for d in range(2):
        down_all[2 * me + d] = down_ref[:, d * half : (d + 1) * half]
    for copy in tails:
        copy.wait_recv()

    blocks = tokens // WINDOW
    heads_local = q_ref.shape[1] // HEAD
    group = heads_local // (k_ref.shape[1] // HEAD)

    def windows(first, last):
        @pl.loop(first, last)
        def _(i):
            start = pl.multiple_of(i * WINDOW, WINDOW)
            rows, span = pl.ds(start, WINDOW), pl.ds(start, 2 * WINDOW)
            q_index = lax.broadcasted_iota(jnp.int32, (WINDOW, 2 * WINDOW), 0)
            k_index = lax.broadcasted_iota(jnp.int32, (WINDOW, 2 * WINDOW), 1)
            dist = q_index + WINDOW - k_index
            key_pos = me * tokens + start - WINDOW + k_index
            valid = (dist >= 0) & (dist < WINDOW) & (key_pos >= 0)
            far = dist.astype(jnp.float32)
            for h in range(heads_local):
                columns = slice(h * HEAD, (h + 1) * HEAD)
                shared = slice(h // group * HEAD, (h // group + 1) * HEAD)
                logits = lax.dot_general(
                    q_ref[rows, columns], key_ext[span, shared], (((1,), (1,)), ((), ())),
                    preferred_element_type=jnp.float32,
                ) * HEAD ** (-0.5)
                logits = jnp.where(valid, logits - slopes_ref[h] * far, neg_big)
                sink = sinks_ref[h]
                top = jnp.maximum(jnp.max(logits, axis=-1, keepdims=True), sink)
                probs = jnp.exp(logits - top)
                denom = jnp.sum(probs, axis=-1, keepdims=True) + jnp.exp(sink - top)
                weight = (probs / denom).astype(jnp.bfloat16)
                attended[rows, columns] = jnp.dot(
                    weight, val_ext[span, shared], preferred_element_type=jnp.float32
                ).astype(jnp.bfloat16)

    windows(0, blocks // 2)
    serve(0, 0, 0)
    windows(blocks // 2, blocks)
    serve(0, 0, 1)

    @pl.loop(0, width // (2 * LANES))
    def _(i):
        columns = pl.ds(pl.multiple_of(i * 2 * LANES, 2 * LANES), 2 * LANES)
        mix_ref[:, columns] = jnp.dot(
            attended[...], proj_ref[:, columns], preferred_element_type=jnp.float32
        ).astype(jnp.bfloat16)

    mix_copies = [
        remote(
            mix_ref.at[pl.ds(pl.multiple_of(peer(k) * own_rows, own_rows), own_rows)],
            mix_in.at[k - 1], mix_send.at[k - 1], mix_recv.at[k - 1], (me, peer(k)),
        )
        for k in range(1, m)
    ]
    for copy in mix_copies:
        copy.start()

    early = n // 2
    for s in range(1, early):
        serve_up(s)
    for copy in mix_copies:
        copy.wait_recv()

    @pl.loop(0, own_rows // step_rows)
    def _(i):
        start = pl.multiple_of(i * step_rows, step_rows)
        rows = pl.ds(start, step_rows)
        mine = pl.ds(pl.multiple_of(rank * own_rows + start, step_rows), step_rows)
        mix = mix_ref[mine].astype(jnp.float32)
        for k in range(m - 1):
            mix += mix_in[k, rows].astype(jnp.float32)
        stream = deep_alpha * res_ref[rows].astype(jnp.float32) + mix
        normed[mine] = norm_rows(stream, gains_ref[0:1], biases_ref[0:1]).astype(jnp.bfloat16)

    held = pl.ds(pl.multiple_of(rank * own_rows, own_rows), own_rows)
    row_copies = [
        remote(
            normed.at[held], normed.at[held], row_send.at[k - 1], row_recv.at[k - 1], (me, peer(k))
        )
        for k in range(1, m)
    ]
    for copy in row_copies:
        copy.start()
    for s in range(early, n - 1):
        serve_up(s)
    for copy in row_copies:
        copy.wait_recv()

    tile = 256
    tiles = hidden // tile
    parts = 4

    def upward(first, last):
        @pl.loop(first, last)
        def _(i):
            columns = pl.ds(pl.multiple_of(i * tile, tile), tile)
            made = jnp.dot(normed[...], up_all[:, columns], preferred_element_type=jnp.float32)
            act[:, columns] = jnp.square(jnp.maximum(made, 0.0)).astype(jnp.bfloat16)

    for part in range(parts):
        upward(part * tiles // parts, (part + 1) * tiles // parts)
        if part < 2:
            serve(1, 0, part)

    def owners(j):
        return member(place - j), member(place + j)

    def share(j, k):
        return remote(
            terms.at[j, :, pl.ds(pl.multiple_of(peer(k) * own_rows, own_rows), own_rows)],
            terms_in.at[k - 1, j], sum_send.at[k - 1, j], sum_recv.at[k - 1, j], (me, peer(k)),
        )

    def downward(j):
        for d, owner in enumerate(owners(j)):
            terms[j, d] = jnp.dot(
                act[...], down_all[2 * owner + d], preferred_element_type=jnp.float32
            ).astype(jnp.bfloat16)
        for k in range(1, m):
            share(j, k).start()

    def collect(j):
        for k in range(1, m):
            share(j, k).wait_recv()
        for d, owner in enumerate(owners(j)):
            columns = pl.ds(pl.multiple_of(owner * depth + d * half, half), half)
            block = terms[j, d, held].astype(jnp.float32)
            for k in range(m - 1):
                block += terms_in[k, j, d].astype(jnp.float32)
            total[:, columns] = deep_alpha * normed[held, columns].astype(jnp.float32) + block

    downward(0)
    downward(1)
    for s in range(1, n - 1):
        for c in range(2):
            serve(1, s, c)
        downward(s + 1)
        collect(s - 1)
    collect(n - 2)
    collect(n - 1)

    @pl.loop(0, own_rows // step_rows)
    def _(i):
        rows = pl.ds(pl.multiple_of(i * step_rows, step_rows), step_rows)
        out_ref[rows] = norm_rows(total[rows], gains_ref[1:2], biases_ref[1:2]).astype(jnp.bfloat16)

    for copy in tails + mix_copies + row_copies:
        copy.wait_send()
    for j in range(n):
        for k in range(1, m):
            share(j, k).wait_send()
    for which in range(2):
        for s in range(n - 1):
            for d in range(2):
                for c in range(2):
                    hop(which, s, d, c).wait_send()


def fused_block(
    queries, keys, values, sinks, slopes, out_weight, up_weight, down_weight, residual, gains, biases
):
    n, m = lax.axis_size("sp"), lax.axis_size("tp")
    depth, hidden = up_weight.shape
    half = depth // 2
    tokens = queries.shape[0]
    own_rows, width = residual.shape
    vmem, smem = pl.BlockSpec(memory_space=pltpu.VMEM), pl.BlockSpec(memory_space=pltpu.SMEM)
    bf16, dma = jnp.bfloat16, pltpu.SemaphoreType.DMA
    return pl.pallas_call(
        functools.partial(block_kernel, n, m),
        out_shape=jax.ShapeDtypeStruct(residual.shape, bf16),
        in_specs=[vmem] * 3 + [smem] * 2 + [vmem] * 6,
        out_specs=pl.BlockSpec(memory_space=pltpu.VMEM),
        scratch_shapes=[
            pltpu.VMEM((tokens + WINDOW, keys.shape[1]), bf16),
            pltpu.VMEM((tokens + WINDOW, keys.shape[1]), bf16),
            pltpu.VMEM(queries.shape, bf16),
            pltpu.VMEM((tokens, width), bf16),
            pltpu.VMEM((width, hidden), bf16),
            pltpu.VMEM((2 * n, hidden, half), bf16),
            pltpu.VMEM((m - 1, own_rows, width), bf16),
            pltpu.VMEM((tokens, width), bf16),
            pltpu.VMEM((tokens, hidden), bf16),
            pltpu.VMEM((n, 2, tokens, half), bf16),
            pltpu.VMEM((m - 1, n, 2, own_rows, half), bf16),
            pltpu.VMEM((own_rows, width), jnp.float32),
            dma((2,)),
            dma((2,)),
            dma((2, n - 1, 2, 2)),
            dma((2, n - 1, 2, 2)),
            dma((m - 1,)),
            dma((m - 1,)),
            dma((m - 1,)),
            dma((m - 1,)),
            dma((m - 1, n)),
            dma((m - 1, n)),
        ],
        compiler_params=pltpu.CompilerParams(
            collective_id=0, has_side_effects=True, vmem_limit_bytes=60 * 1024 * 1024
        ),
    )(
        queries, keys, values, sinks, slopes, out_weight, up_weight, down_weight, residual, gains,
        biases,
    )


def on_device(
    queries, keys, values, residual, sinks, out_weight, up_weight, down_weight, gains, biases
):
    tokens = queries.shape[0]
    rank_tp = lax.axis_index("tp")
    if up_weight.shape[0] % (2 * LANES) == 0 and lax.axis_size("sp") % 2 == 0:
        heads_local = sinks.shape[0]
        heads = (jnp.arange(heads_local, dtype=jnp.int32) + rank_tp * heads_local).astype(jnp.float32)
        slopes = jnp.exp2(-8.0 * (heads + 1.0) / HEADS)
        return fused_block(
            queries, keys, values, sinks, slopes, out_weight, up_weight, down_weight, residual,
            gains, biases,
        )
    tails = jnp.stack([keys[tokens - WINDOW :], values[tokens - WINDOW :]])
    before = from_behind(tails, "sp", 1)
    offset = lax.axis_index("sp") * tokens
    attended = attend(queries, keys, values, before, sinks, offset, rank_tp)
    part = jnp.dot(attended, out_weight, preferred_element_type=jnp.float32).astype(jnp.bfloat16)
    up_full, down_full = (
        lax.all_gather(up_weight, "sp", axis=0, tiled=True),
        lax.all_gather(down_weight, "sp", axis=1, tiled=True),
    )
    mix = lax.psum_scatter(
        part,
        "tp",
        scatter_dimension=0,
        tiled=True,
    ).astype(jnp.float32)
    normed = layer_norm(deep_alpha * residual.astype(jnp.float32) + mix, gains[0], biases[0])
    whole = lax.all_gather(normed, "tp", axis=0, tiled=True)
    upward = jnp.dot(whole, up_full, preferred_element_type=jnp.float32)
    act = jnp.square(jax.nn.relu(upward)).astype(jnp.bfloat16)
    terms = jnp.dot(act, down_full, preferred_element_type=jnp.float32)
    ffn = lax.psum_scatter(
        terms.astype(jnp.bfloat16), "tp", scatter_dimension=0, tiled=True
    ).astype(jnp.float32)
    return layer_norm(deep_alpha * normed.astype(jnp.float32) + ffn, gains[1], biases[1])


def solution(mesh):
    return jax.shard_map(
        on_device,
        mesh=mesh,
        in_specs=(
            P("sp", "tp"),
            P("sp", "tp"),
            P("sp", "tp"),
            P(("sp", "tp"), None),
            P("tp"),
            P("tp", None),
            P("sp", "tp"),
            P("tp", "sp"),
            P(),
            P(),
        ),
        out_specs=P(("sp", "tp"), None),
        check_vma=False,
    )
```

profile of v0, /device:TPU:1, one launch (start us, length us, event | category | flops | bytes accessed | tf_op | source)
XLA Modules:
  0.0 179.3 jit_solution(12671939969960642474)
XLA Ops:
  0.0 0.5 multiply_exponential_fusion.slopes_ref
  0.5 176.7 %shard_map.100 = bf16[192,2048]{1,0:T(8,128)(2,1)} custom-call(bf16[768,384]{1,0:T(8,128)(2,1)} %q_ref.1, bf16[768,128]{1,0:T(8,128)(2,1)} %k_ref.1, bf16[768,128]{1,0:T(8,128)(2,1)} %v_ref.1, f32[3]{0:T(128)} %sinks_ref.1, f32[3]{0:T(128)} %multiply_exponential_fusion.slopes_ref, bf16[384,2048]{1,0:T(8,128)(2,1)} %proj_ref.1, bf16[256,2048]{1,0:T(8,128)(2,1)} %up_ref.1, ...), custom_call_target="tpu_custom_call" | custom-call | tf_op jit(solution)/shard_map/pallas_call | solution.py:344
  177.2 2.1 %copy.12 = bf16[192,2048]{1,0:T(8,128)(2,1)} copy(bf16[192,2048]{1,0:T(8,128)(2,1)} %shard_map.100) | data formatting | bytes 1572864
where the time goes:
time: 181 us; the launch traced here: 179 us
  Pallas kernels  177 us (98%)
  local copies, waits for them, and re-layouts  2.09 us (1%)
    pallas_call x1, Pallas kernels, fused_block(): pl.pallas_call(functools.partial(block_kernel, n, m), out_shape=jax.Shape...  177 us

commit v1 on v0

v1 whole, which is shorter than its diff:
```python
import functools

import jax
import jax.numpy as jnp
from jax import lax
from jax.experimental import pallas as pl
from jax.experimental.pallas import tpu as pltpu
from jax.sharding import PartitionSpec as P

HEADS = 12
HEAD = 128
WINDOW = 128


deep_alpha = 1.6817928
norm_eps = 1e-05
neg_big = -1e30


def from_behind(block, axis, distance):
    devices = range(lax.axis_size(axis))
    route = [(i - distance, i) for i in devices if i - distance in devices]
    return lax.ppermute(block, axis, route)


def layer_norm(stream, gain, bias):
    mean = jnp.mean(stream, axis=-1, keepdims=True)
    spread = jnp.mean(jnp.square(stream - mean), axis=-1, keepdims=True)
    return ((stream - mean) * lax.rsqrt(spread + norm_eps) * gain + bias).astype(jnp.bfloat16)


def attend(queries, keys, values, before, sinks, offset, rank_tp):
    tokens = keys.shape[0]
    kv_local = keys.shape[1] // HEAD
    heads_local = sinks.shape[0]
    group = heads_local // kv_local
    blocks = tokens // WINDOW
    q_blocks = queries.reshape(blocks, WINDOW, kv_local, group, HEAD)
    key_ext = jnp.concatenate([before[0], keys], axis=0).reshape(tokens + WINDOW, kv_local, HEAD)
    val_ext = jnp.concatenate([before[1], values], axis=0).reshape(tokens + WINDOW, kv_local, HEAD)
    key_win = jnp.concatenate(
        [
            key_ext[:tokens].reshape(blocks, WINDOW, kv_local, HEAD),
            key_ext[WINDOW:].reshape(blocks, WINDOW, kv_local, HEAD),
        ],
        axis=1,
    )
    val_win = jnp.concatenate(
        [
            val_ext[:tokens].reshape(blocks, WINDOW, kv_local, HEAD),
            val_ext[WINDOW:].reshape(blocks, WINDOW, kv_local, HEAD),
        ],
        axis=1,
    )
    logits = jnp.einsum(
        "nqkgd,nskd->nkgqs", q_blocks, key_win, preferred_element_type=jnp.float32
    ) * HEAD ** (-0.5)
    q_index = jnp.arange(WINDOW, dtype=jnp.int32)[:, None]
    k_index = jnp.arange(2 * WINDOW, dtype=jnp.int32)[None, :]
    dist = q_index + WINDOW - k_index
    block_id = jnp.arange(blocks, dtype=jnp.int32)[:, None, None]
    key_pos = offset + block_id * WINDOW - WINDOW + k_index
    valid = (dist >= 0) & (dist < WINDOW) & (key_pos >= 0)
    heads = (jnp.arange(heads_local, dtype=jnp.int32) + rank_tp * heads_local).astype(jnp.float32)
    slopes = jnp.exp2(-8.0 * (heads + 1.0) / HEADS).reshape(kv_local, group)[:, :, None, None]
    logits = logits - slopes * dist.astype(jnp.float32)
    logits = jnp.where(valid[:, None, None], logits, neg_big)
    sink = sinks.reshape(kv_local, group)[:, :, None, None]
    top = jnp.maximum(jnp.max(logits, axis=-1, keepdims=True), sink)
    probs = jnp.exp(logits - top)
    denom = jnp.sum(probs, axis=-1, keepdims=True) + jnp.exp(sink - top)
    weight = (probs / denom).astype(jnp.bfloat16)
    attended = jnp.einsum("nkgqs,nskd->nqkgd", weight, val_win, preferred_element_type=jnp.float32)
    return attended.astype(jnp.bfloat16).reshape(tokens, heads_local * HEAD)


MESH = pl.DeviceIdType.MESH
LANES = 128


def norm_rows(stream, gain, bias):
    mean = jnp.mean(stream, axis=-1, keepdims=True)
    spread = jnp.mean(jnp.square(stream - mean), axis=-1, keepdims=True)
    return (stream - mean) * lax.rsqrt(spread + norm_eps) * gain + bias


ROWS_Y, LAYERS, CORES, SIDES = 2, 4, 2, 2
PIECES = 2
ROW_PARTS = 2


def fits(tokens, up_weight):
    depth, hidden = up_weight.shape
    return (
        lax.axis_size("sp") == ROWS_Y * LAYERS
        and lax.axis_size("tp") == CORES * SIDES
        and depth % (2 * LANES) == 0
        and hidden % (2 * PIECES * LANES) == 0
        and tokens % (2 * WINDOW) == 0
        and tokens % (SIDES * CORES * ROW_PARTS * 32) == 0
    )


def block_kernel(
    n, m, q_ref, k_ref, v_ref, sinks_ref, slopes_ref, proj_ref, up_ref, down_ref, res_ref,
    gains_ref, biases_ref, out_ref,
    key_ext, val_ext, attended, att_in, proj_in, mix_out, mix_own, mix_in, up_all, down_all,
    normed_own, normed, act, terms, cross_in, joined, terms_in, total,
    tail_send, tail_recv, proj_send, proj_recv, att_send, att_recv, mix_send, mix_recv,
    main_send, extra_send, pass_send, z_recv, first_send, y_send, y_recv, all_send, all_recv,
    d_send, d_recv, row_send, row_recv, fwd_send, out_send, cross_send, cross_recv, join_send, out_recv,
):
    me, rank = lax.axis_index("sp"), lax.axis_index("tp")
    depth, hidden = up_ref.shape
    own_rows, width = res_ref.shape
    tokens = q_ref.shape[0]
    q_width = q_ref.shape[1]
    side_rows = tokens // SIDES
    y, z = lax.rem(me, ROWS_Y), lax.div(me, ROWS_Y)
    x, c = lax.div(rank, CORES), lax.rem(rank, CORES)
    half, zl = lax.div(z, 2), lax.rem(z, 2)
    oy, ox, oc = 1 - y, 1 - x, 1 - c
    oz = z + 1 - 2 * zl
    u = zl + half - 2 * zl * half
    step_rows = 32

    home = c == zl
    away = c != zl
    h1 = 1 - lax.rem(c + zl, 2)

    def layer(w):
        return w + half * (LAYERS - 1 - 2 * w)

    def source(k):
        return layer(u if k == 0 else 1 - u if k == 1 else k)

    def at(x_, y_, z_, c_):
        return (z_ * ROWS_Y + y_, x_ * CORES + c_)

    barrier = pltpu.get_barrier_semaphore()
    partners = [at(x, y, z, oc)]
    for k in range(1, LAYERS):
        for core in range(CORES):
            partners.append(at(x, y, lax.rem(z + k, LAYERS), core))
    for core in range(CORES):
        partners.append(at(x, oy, z, core))
        partners.append(at(ox, y, z, core))
    partners.append(at(x, oy, lax.rem(z + 2 * y - 1 + LAYERS, LAYERS), c))
    for there in partners:
        pl.semaphore_signal(barrier, inc=1, device_id=there, device_id_type=MESH)
    pl.semaphore_wait(barrier, len(partners))

    def remote(source, target, send, recv, device):
        return pltpu.make_async_remote_copy(
            src_ref=source, dst_ref=target, send_sem=send, recv_sem=recv,
            device_id=device, device_id_type=MESH,
        )

    def held(kind, s, h, p):
        if kind == 0:
            rows = depth // (2 * PIECES)
            off = s * depth + h * (depth // 2) + p * rows
            return up_all.at[pl.ds(pl.multiple_of(off, rows), rows)]
        rows = hidden // (2 * PIECES)
        off = h * (hidden // 2) + p * rows
        return down_all.at[s, pl.ds(pl.multiple_of(off, rows), rows)]

    def own_piece(kind, h, p):
        ref = up_ref if kind == 0 else down_ref
        rows = ref.shape[0] // (2 * PIECES)
        return ref.at[pl.ds(h * (ref.shape[0] // 2) + p * rows, rows)]

    w_main = h1 * (u + 2) + (1 - h1) * (u + 1)
    k_main = h1 * (3 - u) + (1 - h1) * (1 + u)

    def main(kind, h, p):
        return remote(
            own_piece(kind, h, p), held(kind, me, h, p), main_send.at[kind, h, p],
            z_recv.at[kind, k_main, p], at(x, y, layer(w_main), h),
        )

    def extra(kind, h, p):
        return remote(
            own_piece(kind, h, p), held(kind, me, h, p), extra_send.at[kind, h, p],
            z_recv.at[kind, 1, p], at(x, y, layer(0), h),
        )

    extra_here = (u == 1) & away

    def column(k, other):
        return source(k) * ROWS_Y + (oy if other else y)

    def z_piece(kind, k, p):
        ref = held(kind, column(k, 0), c, p)
        return remote(ref, ref, pass_send.at[kind, p], z_recv.at[kind, k, p], at(x, y, z, oc))

    def passed(kind, p):
        ref = held(kind, column(1, 0), c, p)
        return remote(
            ref, ref, pass_send.at[kind, p], z_recv.at[kind, 3, p], at(x, y, layer(3), c)
        )

    def first(kind, h, p):
        return remote(
            own_piece(kind, h, p), held(kind, me, h, p), first_send.at[kind, h, p],
            y_recv.at[kind, 0, p], at(x, oy, z, h),
        )

    def y_out(kind, k, p):
        ref = held(kind, column(k, 0), c, p)
        return remote(
            ref, ref, y_send.at[kind, k, p], y_recv.at[kind, k, p], at(x, oy, z, c)
        )

    def y_in(kind, k, p):
        ref = held(kind, column(k, 1), c, p)
        return remote(
            ref, ref, y_send.at[kind, k, p], y_recv.at[kind, k, p], at(x, oy, z, c)
        )

    def across(kind, other, k, p, h):
        ref = held(kind, column(k, other), h, p)
        return remote(
            ref, ref, d_send.at[kind, other, k, p], d_recv.at[kind, other, k, p],
            at(x, y, z, oc),
        )

    def whole(kind):
        ref = up_ref if kind == 0 else down_ref
        if kind == 0:
            target = up_all.at[pl.ds(pl.multiple_of(me * depth, depth), depth)]
        else:
            target = down_all.at[me]
        return remote(ref, target, all_send.at[kind], all_recv.at[kind], at(x, y, z, oc))

    def launch_local(kind):
        @pl.when(home)
        def _():
            whole(kind).start()
            for p in range(PIECES):
                for h in range(2):
                    first(kind, h, p).start()

    def launch_main(kind):
        for p in range(PIECES):
            for h in range(2):
                main(kind, h, p).start()

    def launch_extra(kind):
        @pl.when(extra_here)
        def _():
            for p in range(PIECES):
                for h in range(2):
                    extra(kind, h, p).start()

    def serve_z(kind, k):
        for p in range(PIECES):
            z_piece(kind, k, p).wait_recv()
            if k == 1:
                @pl.when(u == 1)
                def _():
                    passed(kind, p).start()
            y_out(kind, k, p).start()
            across(kind, 0, k, p, c).start()

    def serve_y(kind, k):
        for p in range(PIECES):
            y_in(kind, k, p).wait_recv()
            across(kind, 1, k, p, c).start()

    def need(kind, other, k):
        if k == 0 and not other:
            @pl.when(away)
            def _():
                whole(kind).wait_recv()
            return
        for p in range(PIECES):
            across(kind, other, k, p, oc).wait_recv()

    after = lax.rem(me + 1, n)
    tails = [
        remote(
            ref.at[pl.ds(tokens - WINDOW, WINDOW)], ext.at[pl.ds(0, WINDOW)],
            tail_send.at[i], tail_recv.at[i], (after, rank),
        )
        for i, (ref, ext) in enumerate(((k_ref, key_ext), (v_ref, val_ext)))
    ]
    for copy in tails:
        copy.start()
    launch_main(0)
    launch_extra(0)
    proj_copy = remote(proj_ref, proj_in, proj_send.at[0], proj_recv.at[0], at(x, y, z, oc))
    proj_copy.start()
    launch_local(0)
    key_ext[WINDOW:] = k_ref[...]
    val_ext[WINDOW:] = v_ref[...]

    @pl.when(home)
    def _():
        up_all[pl.ds(pl.multiple_of(me * depth, depth), depth)] = up_ref[...]
        down_all[me] = down_ref[...]

    for copy in tails:
        copy.wait_recv()

    blocks = tokens // WINDOW
    heads_local = q_width // HEAD
    group = heads_local // (k_ref.shape[1] // HEAD)

    def windows(first_block, count):
        @pl.loop(0, count)
        def _(i):
            start = pl.multiple_of((first_block + i) * WINDOW, WINDOW)
            rows, span = pl.ds(start, WINDOW), pl.ds(start, 2 * WINDOW)
            q_index = lax.broadcasted_iota(jnp.int32, (WINDOW, 2 * WINDOW), 0)
            k_index = lax.broadcasted_iota(jnp.int32, (WINDOW, 2 * WINDOW), 1)
            dist = q_index + WINDOW - k_index
            key_pos = me * tokens + start - WINDOW + k_index
            valid = (dist >= 0) & (dist < WINDOW) & (key_pos >= 0)
            far = dist.astype(jnp.float32)
            for h in range(heads_local):
                columns = slice(h * HEAD, (h + 1) * HEAD)
                shared = slice(h // group * HEAD, (h // group + 1) * HEAD)
                logits = lax.dot_general(
                    q_ref[rows, columns], key_ext[span, shared], (((1,), (1,)), ((), ())),
                    preferred_element_type=jnp.float32,
                ) * HEAD ** (-0.5)
                logits = jnp.where(valid, logits - slopes_ref[h] * far, neg_big)
                sink = sinks_ref[h]
                top = jnp.maximum(jnp.max(logits, axis=-1, keepdims=True), sink)
                probs = jnp.exp(logits - top)
                denom = jnp.sum(probs, axis=-1, keepdims=True) + jnp.exp(sink - top)
                weight = (probs / denom).astype(jnp.bfloat16)
                attended[rows, columns] = jnp.dot(
                    weight, val_ext[span, shared], preferred_element_type=jnp.float32
                ).astype(jnp.bfloat16)

    def rows_of(side, core):
        start = side * side_rows + core * own_rows
        return pl.ds(pl.multiple_of(start, own_rows), own_rows)

    def swap(i, side):
        return remote(
            attended.at[rows_of(side, oc)], att_in.at[i], att_send.at[i], att_recv.at[i],
            at(x, y, z, oc),
        )

    tile = 2 * LANES

    def project(i, side, target):
        @pl.loop(0, width // tile)
        def _(j):
            columns = pl.ds(pl.multiple_of(j * tile, tile), tile)
            target[:, columns] = (
                jnp.dot(
                    attended[rows_of(side, c)], proj_ref[:, columns],
                    preferred_element_type=jnp.float32,
                )
                + jnp.dot(att_in[i], proj_in[:, columns], preferred_element_type=jnp.float32)
            ).astype(target.dtype)

    part_rows = own_rows // ROW_PARTS

    def mix_copy(p):
        rows = pl.ds(p * part_rows, part_rows)
        return remote(
            mix_out.at[rows], mix_in.at[rows], mix_send.at[p], mix_recv.at[p], at(ox, y, z, c)
        )

    windows(ox * (blocks // 2), blocks // 2)
    swap(0, ox).start()
    proj_copy.wait_recv()
    swap(0, ox).wait_recv()
    project(0, ox, mix_out)
    for p in range(ROW_PARTS):
        mix_copy(p).start()
    serve_y(0, 0)
    windows(x * (blocks // 2), blocks // 2)
    swap(1, x).start()
    serve_z(0, 1)
    swap(1, x).wait_recv()
    project(1, x, mix_own)
    serve_y(0, 1)

    def rank_rows(r, p):
        start = r * own_rows + p * part_rows
        return pl.ds(pl.multiple_of(start, part_rows), part_rows)

    def row_copy(t, p):
        source_ref, rows = normed_own.at[pl.ds(p * part_rows, part_rows)], rank_rows(rank, p)
        there = [at(x, y, z, oc), at(ox, y, z, zl), at(x, y, oz, zl)][t]
        return remote(
            source_ref, normed.at[rows], row_send.at[t, p], row_recv.at[rank, p], there
        )

    def row_in(side, core, p):
        r = side * CORES + core
        ref = normed.at[rank_rows(r, p)]
        return remote(ref, ref, fwd_send.at[core, p], row_recv.at[r, p], at(ox, y, z, c))

    for p in range(ROW_PARTS):
        mix_copy(p).wait_recv()

        @pl.loop(0, part_rows // step_rows)
        def _(i):
            start = pl.multiple_of(p * part_rows + i * step_rows, step_rows)
            rows = pl.ds(start, step_rows)
            mix = mix_own[rows] + mix_in[rows].astype(jnp.float32)
            stream = deep_alpha * res_ref[rows].astype(jnp.float32) + mix
            made = norm_rows(stream, gains_ref[0:1], biases_ref[0:1]).astype(jnp.bfloat16)
            normed_own[rows] = made

            @pl.when(home)
            def _():
                mine = pl.ds(pl.multiple_of(rank * own_rows + start, step_rows), step_rows)
                normed[mine] = made

        row_copy(2, p).start()
        row_copy(1, p).start()

        @pl.when(away)
        def _():
            row_copy(0, p).start()

    serve_z(0, 2)
    launch_main(1)
    launch_extra(1)
    launch_local(1)
    serve_y(0, 2)

    @pl.when(away)
    def _():
        for p in range(ROW_PARTS):
            for core in range(CORES):
                row_in(x, core, p).wait_recv()
                row_in(x, core, p).start()

    serve_z(0, 3)
    serve_y(0, 3)
    serve_z(1, 1)
    for k in range(LAYERS):
        for other in range(2):
            need(0, other, k)

    for p in range(ROW_PARTS):
        for core in range(CORES):
            row_in(ox, core, p).wait_recv()

        @pl.when(home)
        def _():
            row_in(x, oc, p).wait_recv()

    tiles = hidden // tile

    def upward(first, last):
        @pl.loop(first, last)
        def _(i):
            columns = pl.ds(pl.multiple_of(i * tile, tile), tile)
            made = jnp.dot(normed[...], up_all[:, columns], preferred_element_type=jnp.float32)
            act[:, columns] = jnp.square(jnp.maximum(made, 0.0)).astype(jnp.bfloat16)

    parts = 4
    for part in range(parts):
        upward(part * tiles // parts, (part + 1) * tiles // parts)
        if part == 0:
            serve_y(1, 0)
        elif part == 1:
            serve_y(1, 1)
        elif part == 2:
            serve_z(1, 2)
        else:
            serve_y(1, 2)

    steps = 2 * LAYERS

    def out_copy(i, t):
        r = [x * CORES + oc, ox * CORES, ox * CORES + 1][t]
        rows = pl.ds(pl.multiple_of(r * own_rows, own_rows), own_rows)
        there = [at(x, y, z, oc), at(ox, y, z, 0), at(ox, y, z, 1)][t]
        slot = 0 if t == 0 else 1
        return remote(
            terms.at[i, rows], terms_in.at[slot, i], out_send.at[i, t], out_recv.at[slot, i], there
        )

    def cross_copy(i):
        rows = pl.ds(pl.multiple_of(ox * side_rows, side_rows), side_rows)
        return remote(
            terms.at[i, rows], cross_in.at[i], cross_send.at[i], cross_recv.at[i], at(ox, y, z, c)
        )

    def join_copy(i, core):
        return remote(
            joined.at[i, pl.ds(core * own_rows, own_rows)], terms_in.at[2, i],
            join_send.at[i, core], out_recv.at[2, i], at(x, y, oz, core),
        )

    held_rows = pl.ds(pl.multiple_of(rank * own_rows, own_rows), own_rows)

    def downward(i):
        s = column(i // 2, i % 2)
        terms[i] = jnp.dot(
            act[...], down_all[s], preferred_element_type=jnp.float32
        ).astype(jnp.bfloat16)

        @pl.when(home)
        def _():
            for t in range(3):
                out_copy(i, t).start()
            terms_in[0, i] = terms[i, held_rows]

        @pl.when(away)
        def _():
            cross_copy(i).start()

    def join(i):
        @pl.when(away)
        def _():
            cross_copy(i).wait_recv()
            rows = pl.ds(pl.multiple_of(x * side_rows, side_rows), side_rows)
            joined[i] = (
                terms[i, rows].astype(jnp.float32) + cross_in[i].astype(jnp.float32)
            ).astype(jnp.bfloat16)
            for core in range(CORES):
                join_copy(i, core).start()

    def collect(k):
        for other in range(2):
            i = 2 * k + other
            i2 = 2 * (1 - k if k < 2 else k) + other

            @pl.when(away)
            def _():
                out_copy(i, 0).wait_recv()

            out_copy(i, 1).wait_recv()
            join_copy(i2, 0).wait_recv()
            columns = pl.ds(pl.multiple_of(column(k, other) * depth, depth), depth)
            block = terms_in[0, i].astype(jnp.float32)
            block += terms_in[1, i].astype(jnp.float32)
            block += terms_in[2, i2].astype(jnp.float32)
            total[:, columns] = deep_alpha * normed_own[:, columns].astype(jnp.float32) + block

    for i in range(steps):
        k, other = i // 2, i % 2
        if i == 6:
            serve_z(1, 3)
        if i == 7:
            serve_y(1, 3)
        need(1, other, k)
        downward(i)
        if i >= 1:
            join(i - 1)
        if i == 4:
            collect(0)
        if i == 5:
            collect(1)
    join(steps - 1)
    collect(2)
    collect(3)

    @pl.loop(0, own_rows // step_rows)
    def _(i):
        rows = pl.ds(pl.multiple_of(i * step_rows, step_rows), step_rows)
        out_ref[rows] = norm_rows(total[rows], gains_ref[1:2], biases_ref[1:2]).astype(jnp.bfloat16)

    for copy in tails:
        copy.wait_send()
    proj_copy.wait_send()
    swap(0, ox).wait_send()
    swap(1, x).wait_send()
    for p in range(ROW_PARTS):
        mix_copy(p).wait_send()
        row_copy(1, p).wait_send()
        row_copy(2, p).wait_send()
    for kind in range(2):
        for p in range(PIECES):
            for h in range(2):
                main(kind, h, p).wait_send()
            for k in range(LAYERS):
                if k > 0:
                    y_out(kind, k, p).wait_send()
                    across(kind, 0, k, p, c).wait_send()
                across(kind, 1, k, p, c).wait_send()

    @pl.when(extra_here)
    def _():
        for kind in range(2):
            for p in range(PIECES):
                for h in range(2):
                    extra(kind, h, p).wait_send()

    @pl.when(u == 1)
    def _():
        for kind in range(2):
            for p in range(PIECES):
                passed(kind, p).wait_send()

    @pl.when(home)
    def _():
        for kind in range(2):
            whole(kind).wait_send()
            for p in range(PIECES):
                for h in range(2):
                    first(kind, h, p).wait_send()
        for i in range(steps):
            for t in range(3):
                out_copy(i, t).wait_send()

    @pl.when(away)
    def _():
        for p in range(ROW_PARTS):
            row_copy(0, p).wait_send()
            for core in range(CORES):
                row_in(x, core, p).wait_send()
        for i in range(steps):
            cross_copy(i).wait_send()
            for core in range(CORES):
                join_copy(i, core).wait_send()


def fused_block(
    queries, keys, values, sinks, slopes, out_weight, up_weight, down_weight, residual, gains, biases
):
    n, m = lax.axis_size("sp"), lax.axis_size("tp")
    depth, hidden = up_weight.shape
    tokens = queries.shape[0]
    own_rows, width = residual.shape
    side_rows, steps = tokens // SIDES, 2 * LAYERS
    vmem, smem = pl.BlockSpec(memory_space=pltpu.VMEM), pl.BlockSpec(memory_space=pltpu.SMEM)
    bf16, dma = jnp.bfloat16, pltpu.SemaphoreType.DMA
    return pl.pallas_call(
        functools.partial(block_kernel, n, m),
        out_shape=jax.ShapeDtypeStruct(residual.shape, bf16),
        in_specs=[vmem] * 3 + [smem] * 2 + [vmem] * 6,
        out_specs=pl.BlockSpec(memory_space=pltpu.VMEM),
        scratch_shapes=[
            pltpu.VMEM((tokens + WINDOW, keys.shape[1]), bf16),
            pltpu.VMEM((tokens + WINDOW, keys.shape[1]), bf16),
            pltpu.VMEM(queries.shape, bf16),
            pltpu.VMEM((SIDES, own_rows, queries.shape[1]), bf16),
            pltpu.VMEM(out_weight.shape, bf16),
            pltpu.VMEM((own_rows, width), bf16),
            pltpu.VMEM((own_rows, width), jnp.float32),
            pltpu.VMEM((own_rows, width), bf16),
            pltpu.VMEM((width, hidden), bf16),
            pltpu.VMEM((n, hidden, depth), bf16),
            pltpu.VMEM((own_rows, width), bf16),
            pltpu.VMEM((tokens, width), bf16),
            pltpu.VMEM((tokens, hidden), bf16),
            pltpu.VMEM((steps, tokens, depth), bf16),
            pltpu.VMEM((steps, side_rows, depth), bf16),
            pltpu.VMEM((steps, side_rows, depth), bf16),
            pltpu.VMEM((3, steps, own_rows, depth), bf16),
            pltpu.VMEM((own_rows, width), jnp.float32),
            dma((2,)),
            dma((2,)),
            dma((1,)),
            dma((1,)),
            dma((SIDES,)),
            dma((SIDES,)),
            dma((ROW_PARTS,)),
            dma((ROW_PARTS,)),
            dma((2, 2, PIECES)),
            dma((2, 2, PIECES)),
            dma((2, PIECES)),
            dma((2, LAYERS, PIECES)),
            dma((2, 2, PIECES)),
            dma((2, LAYERS, PIECES)),
            dma((2, LAYERS, PIECES)),
            dma((2,)),
            dma((2,)),
            dma((2, 2, LAYERS, PIECES)),
            dma((2, 2, LAYERS, PIECES)),
            dma((3, ROW_PARTS)),
            dma((m, ROW_PARTS)),
            dma((CORES, ROW_PARTS)),
            dma((steps, 3)),
            dma((steps,)),
            dma((steps,)),
            dma((steps, CORES)),
            dma((3, steps)),
        ],
        compiler_params=pltpu.CompilerParams(
            collective_id=0, has_side_effects=True, vmem_limit_bytes=60 * 1024 * 1024
        ),
    )(
        queries, keys, values, sinks, slopes, out_weight, up_weight, down_weight, residual, gains,
        biases,
    )


def on_device(
    queries, keys, values, residual, sinks, out_weight, up_weight, down_weight, gains, biases
):
    tokens = queries.shape[0]
    rank_tp = lax.axis_index("tp")
    if fits(tokens, up_weight):
        heads_local = sinks.shape[0]
        heads = (jnp.arange(heads_local, dtype=jnp.int32) + rank_tp * heads_local).astype(jnp.float32)
        slopes = jnp.exp2(-8.0 * (heads + 1.0) / HEADS)
        return fused_block(
            queries, keys, values, sinks, slopes, out_weight, up_weight, down_weight, residual,
            gains, biases,
        )
    tails = jnp.stack([keys[tokens - WINDOW :], values[tokens - WINDOW :]])
    before = from_behind(tails, "sp", 1)
    offset = lax.axis_index("sp") * tokens
    attended = attend(queries, keys, values, before, sinks, offset, rank_tp)
    part = jnp.dot(attended, out_weight, preferred_element_type=jnp.float32).astype(jnp.bfloat16)
    up_full, down_full = (
        lax.all_gather(up_weight, "sp", axis=0, tiled=True),
        lax.all_gather(down_weight, "sp", axis=1, tiled=True),
    )
    mix = lax.psum_scatter(
        part,
        "tp",
        scatter_dimension=0,
        tiled=True,
    ).astype(jnp.float32)
    normed = layer_norm(deep_alpha * residual.astype(jnp.float32) + mix, gains[0], biases[0])
    whole = lax.all_gather(normed, "tp", axis=0, tiled=True)
    upward = jnp.dot(whole, up_full, preferred_element_type=jnp.float32)
    act = jnp.square(jax.nn.relu(upward)).astype(jnp.bfloat16)
    terms = jnp.dot(act, down_full, preferred_element_type=jnp.float32)
    ffn = lax.psum_scatter(
        terms.astype(jnp.bfloat16), "tp", scatter_dimension=0, tiled=True
    ).astype(jnp.float32)
    return layer_norm(deep_alpha * normed.astype(jnp.float32) + ffn, gains[1], biases[1])


def solution(mesh):
    return jax.shard_map(
        on_device,
        mesh=mesh,
        in_specs=(
            P("sp", "tp"),
            P("sp", "tp"),
            P("sp", "tp"),
            P(("sp", "tp"), None),
            P("tp"),
            P("tp", None),
            P("sp", "tp"),
            P("tp", "sp"),
            P(),
            P(),
        ),
        out_specs=P(("sp", "tp"), None),
        check_vma=False,
    )
```

time: 181 us -> 172 us (0.950)
  Pallas kernels: 177 us -> 169 us
    pallas_call x1, Pallas kernels: 177 us -> 169 us  [fused_block(): pl.pallas_call(functools.partial(block_kernel, n, m), out_shape=jax.Shape...]
where the time goes in v1:
time: 172 us
  Pallas kernels  169 us (98%)
  local copies, waits for them, and re-layouts  2.09 us (1%)
    pallas_call x1, Pallas kernels, fused_block(): pl.pallas_call(functools.partial(block_kernel, n, m), out_shape=jax.Shape...  169 us

profile of v1, /device:TPU:1, one launch (start us, length us, event | category | flops | bytes accessed | tf_op | source)
XLA Modules:
  0.0 171.9 jit_solution(7489136330371645831)
XLA Ops:
  0.0 0.5 multiply_exponential_fusion.slopes_ref
  0.5 169.3 %shard_map.100 = bf16[192,2048]{1,0:T(8,128)(2,1)} custom-call(bf16[768,384]{1,0:T(8,128)(2,1)} %q_ref.1, bf16[768,128]{1,0:T(8,128)(2,1)} %k_ref.1, bf16[768,128]{1,0:T(8,128)(2,1)} %v_ref.1, f32[3]{0:T(128)} %sinks_ref.1, f32[3]{0:T(128)} %multiply_exponential_fusion.slopes_ref, bf16[384,2048]{1,0:T(8,128)(2,1)} %proj_ref.1, bf16[256,2048]{1,0:T(8,128)(2,1)} %up_ref.1, ...), custom_call_target="tpu_custom_call" | custom-call | tf_op jit(solution)/shard_map/pallas_call | solution.py:631
  169.8 2.1 %copy.12 = bf16[192,2048]{1,0:T(8,128)(2,1)} copy(bf16[192,2048]{1,0:T(8,128)(2,1)} %shard_map.100) | data formatting | bytes 1572864

commit v2 on v1

--- a/solution.py
+++ b/solution.py
@@ -85,7 +85,7 @@
 
 
 ROWS_Y, LAYERS, CORES, SIDES = 2, 4, 2, 2
-PIECES = 2
+PIECES = 1
 ROW_PARTS = 2
 
 
@@ -102,13 +102,12 @@
 
 
 def block_kernel(
-    n, m, q_ref, k_ref, v_ref, sinks_ref, slopes_ref, proj_ref, up_ref, down_ref, res_ref,
-    gains_ref, biases_ref, out_ref,
-    key_ext, val_ext, attended, att_in, proj_in, mix_out, mix_own, mix_in, up_all, down_all,
+    n, m, q_ref, k_ref, v_ref, sinks_ref, gains_ref, biases_ref, proj_hbm, up_ref, down_ref, res_hbm, out_ref,
+    key_ext, val_ext, proj_ref, res_ref, attended, att_in, proj_in, mix_out, mix_own, mix_in, up_all, down_all,
     normed_own, normed, act, terms, cross_in, joined, terms_in, total,
     tail_send, tail_recv, proj_send, proj_recv, att_send, att_recv, mix_send, mix_recv,
     main_send, extra_send, pass_send, z_recv, first_send, y_send, y_recv, all_send, all_recv,
-    d_send, d_recv, row_send, row_recv, fwd_send, out_send, cross_send, cross_recv, join_send, out_recv,
+    d_send, d_recv, row_send, row_recv, fwd_send, out_send, cross_send, cross_recv, join_send, out_recv, local_sem,
 ):
     me, rank = lax.axis_index("sp"), lax.axis_index("tp")
     depth, hidden = up_ref.shape
@@ -273,6 +272,10 @@
             @pl.when(away)
             def _():
                 whole(kind).wait_recv()
+
+            @pl.when(home)
+            def _():
+                own_block(kind).wait()
             return
         for p in range(PIECES):
             across(kind, other, k, p, oc).wait_recv()
@@ -289,23 +292,39 @@
         copy.start()
     launch_main(0)
     launch_extra(0)
-    proj_copy = remote(proj_ref, proj_in, proj_send.at[0], proj_recv.at[0], at(x, y, z, oc))
+    proj_copy = remote(proj_hbm, proj_in, proj_send.at[0], proj_recv.at[0], at(x, y, z, oc))
     proj_copy.start()
     launch_local(0)
+    proj_local = pltpu.make_async_copy(proj_hbm, proj_ref, local_sem.at[0])
+    res_local = pltpu.make_async_copy(res_hbm, res_ref, local_sem.at[1])
+    proj_local.start()
+    res_local.start()
+
+    def own_block(kind):
+        if kind == 0:
+            target = up_all.at[pl.ds(pl.multiple_of(me * depth, depth), depth)]
+            return pltpu.make_async_copy(up_ref, target, local_sem.at[2])
+        return pltpu.make_async_copy(down_ref, down_all.at[me], local_sem.at[3])
+
+    @pl.when(home)
+    def _():
+        own_block(0).start()
+        own_block(1).start()
+
     key_ext[WINDOW:] = k_ref[...]
     val_ext[WINDOW:] = v_ref[...]
-
-    @pl.when(home)
-    def _():
-        up_all[pl.ds(pl.multiple_of(me * depth, depth), depth)] = up_ref[...]
-        down_all[me] = down_ref[...]
-
-    for copy in tails:
-        copy.wait_recv()
 
     blocks = tokens // WINDOW
     heads_local = q_width // HEAD
     group = heads_local // (k_ref.shape[1] // HEAD)
+
+    slopes = [
+        jnp.exp2(
+            jnp.full((1, 2 * WINDOW), -8.0 / HEADS, jnp.float32)
+            * (rank * heads_local + (h + 1)).astype(jnp.float32)
+        )
+        for h in range(heads_local)
+    ]
 
     def windows(first_block, count):
         @pl.loop(0, count)
@@ -325,7 +344,7 @@
                     q_ref[rows, columns], key_ext[span, shared], (((1,), (1,)), ((), ())),
                     preferred_element_type=jnp.float32,
                 ) * HEAD ** (-0.5)
-                logits = jnp.where(valid, logits - slopes_ref[h] * far, neg_big)
+                logits = jnp.where(valid, logits - slopes[h] * far, neg_big)
                 sink = sinks_ref[h]
                 top = jnp.maximum(jnp.max(logits, axis=-1, keepdims=True), sink)
                 probs = jnp.exp(logits - top)
@@ -367,20 +386,23 @@
             mix_out.at[rows], mix_in.at[rows], mix_send.at[p], mix_recv.at[p], at(ox, y, z, c)
         )
 
-    windows(ox * (blocks // 2), blocks // 2)
+    windows(ox * (blocks // 2) + 1, blocks // 2 - 1)
+    for copy in tails:
+        copy.wait_recv()
+    windows(ox * (blocks // 2), 1)
     swap(0, ox).start()
+    proj_local.wait()
     proj_copy.wait_recv()
     swap(0, ox).wait_recv()
     project(0, ox, mix_out)
     for p in range(ROW_PARTS):
         mix_copy(p).start()
-    serve_y(0, 0)
     windows(x * (blocks // 2), blocks // 2)
     swap(1, x).start()
     serve_z(0, 1)
     swap(1, x).wait_recv()
     project(1, x, mix_own)
-    serve_y(0, 1)
+    res_local.wait()
 
     def rank_rows(r, p):
         start = r * own_rows + p * part_rows
@@ -423,10 +445,21 @@
             row_copy(0, p).start()
 
     serve_z(0, 2)
-    launch_main(1)
-    launch_extra(1)
+
+    @pl.when((u == 0) & away)
+    def _():
+        launch_main(1)
+
+    serve_y(0, 0)
+    serve_y(0, 1)
+
+    serve_z(0, 3)
+
+    @pl.when(((u == 1) & away) | ((u == 0) & home))
+    def _():
+        launch_main(1)
+
     launch_local(1)
-    serve_y(0, 2)
 
     @pl.when(away)
     def _():
@@ -435,9 +468,9 @@
                 row_in(x, core, p).wait_recv()
                 row_in(x, core, p).start()
 
-    serve_z(0, 3)
+    launch_extra(1)
+    serve_y(0, 2)
     serve_y(0, 3)
-    serve_z(1, 1)
     for k in range(LAYERS):
         for other in range(2):
             need(0, other, k)
@@ -463,13 +496,11 @@
     for part in range(parts):
         upward(part * tiles // parts, (part + 1) * tiles // parts)
         if part == 0:
-            serve_y(1, 0)
-        elif part == 1:
-            serve_y(1, 1)
-        elif part == 2:
-            serve_z(1, 2)
-        else:
-            serve_y(1, 2)
+            @pl.when((u == 1) & home)
+            def _():
+                launch_main(1)
+
+            serve_z(1, 1)
 
     steps = 2 * LAYERS
 
@@ -540,23 +571,23 @@
             block += terms_in[2, i2].astype(jnp.float32)
             total[:, columns] = deep_alpha * normed_own[:, columns].astype(jnp.float32) + block
 
+    before = {
+        1: [(serve_y, 0)],
+        3: [(serve_z, 2), (serve_y, 1)],
+        5: [(serve_z, 3), (serve_y, 2)],
+        7: [(serve_y, 3)],
+    }
     for i in range(steps):
         k, other = i // 2, i % 2
-        if i == 6:
-            serve_z(1, 3)
-        if i == 7:
-            serve_y(1, 3)
+        for serve, at_k in before.get(i, []):
+            serve(1, at_k)
         need(1, other, k)
         downward(i)
         if i >= 1:
             join(i - 1)
-        if i == 4:
-            collect(0)
-        if i == 5:
-            collect(1)
     join(steps - 1)
-    collect(2)
-    collect(3)
+    for k in range(LAYERS):
+        collect(k)
 
     @pl.loop(0, own_rows // step_rows)
     def _(i):
@@ -619,7 +650,7 @@
 
 
 def fused_block(
-    queries, keys, values, sinks, slopes, out_weight, up_weight, down_weight, residual, gains, biases
+    queries, keys, values, sinks, out_weight, up_weight, down_weight, residual, gains, biases
 ):
     n, m = lax.axis_size("sp"), lax.axis_size("tp")
     depth, hidden = up_weight.shape
@@ -631,11 +662,13 @@
     return pl.pallas_call(
         functools.partial(block_kernel, n, m),
         out_shape=jax.ShapeDtypeStruct(residual.shape, bf16),
-        in_specs=[vmem] * 3 + [smem] * 2 + [vmem] * 6,
+        in_specs=[vmem] * 3 + [smem] + [vmem] * 2 + [pl.BlockSpec(memory_space=pl.ANY)] * 4,
         out_specs=pl.BlockSpec(memory_space=pltpu.VMEM),
         scratch_shapes=[
             pltpu.VMEM((tokens + WINDOW, keys.shape[1]), bf16),
             pltpu.VMEM((tokens + WINDOW, keys.shape[1]), bf16),
+            pltpu.VMEM(out_weight.shape, bf16),
+            pltpu.VMEM(residual.shape, bf16),
             pltpu.VMEM(queries.shape, bf16),
             pltpu.VMEM((SIDES, own_rows, queries.shape[1]), bf16),
             pltpu.VMEM(out_weight.shape, bf16),
@@ -679,13 +712,13 @@
             dma((steps,)),
             dma((steps, CORES)),
             dma((3, steps)),
+            dma((4,)),
         ],
         compiler_params=pltpu.CompilerParams(
             collective_id=0, has_side_effects=True, vmem_limit_bytes=60 * 1024 * 1024
         ),
     )(
-        queries, keys, values, sinks, slopes, out_weight, up_weight, down_weight, residual, gains,
-        biases,
+        queries, keys, values, sinks, gains, biases, out_weight, up_weight, down_weight, residual,
     )
 
 
@@ -695,12 +728,8 @@
     tokens = queries.shape[0]
     rank_tp = lax.axis_index("tp")
     if fits(tokens, up_weight):
-        heads_local = sinks.shape[0]
-        heads = (jnp.arange(heads_local, dtype=jnp.int32) + rank_tp * heads_local).astype(jnp.float32)
-        slopes = jnp.exp2(-8.0 * (heads + 1.0) / HEADS)
         return fused_block(
-            queries, keys, values, sinks, slopes, out_weight, up_weight, down_weight, residual,
-            gains, biases,
+            queries, keys, values, sinks, out_weight, up_weight, down_weight, residual, gains, biases
         )
     tails = jnp.stack([keys[tokens - WINDOW :], values[tokens - WINDOW :]])
     before = from_behind(tails, "sp", 1)

time: 172 us -> 135 us (0.78)
  the two profiles are of different devices: /device:TPU:1 before, /device:TPU:17 now
where the time goes in v2:
time: 135 us
  Pallas kernels  133 us (99%)
  local copies, waits for them, and re-layouts  2.09 us (2%)
    pallas_call x1, Pallas kernels, fused_block(): pl.pallas_call(functools.partial(block_kernel, n, m), out_shape=jax.Shape...  133 us

profile of v2, /device:TPU:17, one launch (start us, length us, event | category | flops | bytes accessed | tf_op | source)
XLA Modules:
  0.0 135.2 jit_solution(18234045099134887914)
XLA Ops:
  0.0 133.1 %shard_map.100 = bf16[192,2048]{1,0:T(8,128)(2,1)} custom-call(bf16[768,384]{1,0:T(8,128)(2,1)} %q_ref.1, bf16[768,128]{1,0:T(8,128)(2,1)} %k_ref.1, bf16[768,128]{1,0:T(8,128)(2,1)} %v_ref.1, f32[3]{0:T(128)} %sinks_ref.1, f32[2,2048]{1,0:T(2,128)} %gains_ref.1, f32[2,2048]{1,0:T(2,128)} %biases_ref.1, bf16[384,2048]{1,0:T(8,128)(2,1)} %proj_hbm.1, ...), custom_call_target="tpu_custom_call" | custom-call | tf_op jit(solution)/shard_map/pallas_call | solution.py:662
  133.1 2.1 %copy.12 = bf16[192,2048]{1,0:T(8,128)(2,1)} copy(bf16[192,2048]{1,0:T(8,128)(2,1)} %shard_map.100) | data formatting | bytes 1572864

commit v3 on v2

--- a/solution.py
+++ b/solution.py
@@ -85,7 +85,7 @@
 
 
 ROWS_Y, LAYERS, CORES, SIDES = 2, 4, 2, 2
-PIECES = 1
+PIECES = (1, 2)
 ROW_PARTS = 2
 
 
@@ -95,15 +95,15 @@
         lax.axis_size("sp") == ROWS_Y * LAYERS
         and lax.axis_size("tp") == CORES * SIDES
         and depth % (2 * LANES) == 0
-        and hidden % (2 * PIECES * LANES) == 0
+        and hidden % (2 * max(PIECES) * LANES) == 0
         and tokens % (2 * WINDOW) == 0
         and tokens % (SIDES * CORES * ROW_PARTS * 32) == 0
     )
 
 
 def block_kernel(
-    n, m, q_ref, k_ref, v_ref, sinks_ref, gains_ref, biases_ref, proj_hbm, up_ref, down_ref, res_hbm, out_ref,
-    key_ext, val_ext, proj_ref, res_ref, attended, att_in, proj_in, mix_out, mix_own, mix_in, up_all, down_all,
+    n, m, sinks_ref, gains_ref, biases_ref, q_hbm, k_hbm, v_hbm, proj_hbm, up_ref, down_ref, res_hbm, out_ref,
+    q_ref, key_ext, val_ext, proj_ref, res_ref, attended, att_in, proj_in, mix_out, mix_own, mix_in, up_all, down_all,
     normed_own, normed, act, terms, cross_in, joined, terms_in, total,
     tail_send, tail_recv, proj_send, proj_recv, att_send, att_recv, mix_send, mix_recv,
     main_send, extra_send, pass_send, z_recv, first_send, y_send, y_recv, all_send, all_recv,
@@ -147,6 +147,13 @@
     partners.append(at(x, oy, lax.rem(z + 2 * y - 1 + LAYERS, LAYERS), c))
     for there in partners:
         pl.semaphore_signal(barrier, inc=1, device_id=there, device_id_type=MESH)
+    loads = [
+        pltpu.make_async_copy(k_hbm, key_ext.at[pl.ds(WINDOW, tokens)], local_sem.at[4]),
+        pltpu.make_async_copy(v_hbm, val_ext.at[pl.ds(WINDOW, tokens)], local_sem.at[5]),
+        pltpu.make_async_copy(q_hbm, q_ref, local_sem.at[6]),
+    ]
+    for copy in loads:
+        copy.start()
     pl.semaphore_wait(barrier, len(partners))
 
     def remote(source, target, send, recv, device):
@@ -157,16 +164,16 @@
 
     def held(kind, s, h, p):
         if kind == 0:
-            rows = depth // (2 * PIECES)
+            rows = depth // (2 * PIECES[kind])
             off = s * depth + h * (depth // 2) + p * rows
             return up_all.at[pl.ds(pl.multiple_of(off, rows), rows)]
-        rows = hidden // (2 * PIECES)
+        rows = hidden // (2 * PIECES[kind])
         off = h * (hidden // 2) + p * rows
         return down_all.at[s, pl.ds(pl.multiple_of(off, rows), rows)]
 
     def own_piece(kind, h, p):
         ref = up_ref if kind == 0 else down_ref
-        rows = ref.shape[0] // (2 * PIECES)
+        rows = ref.shape[0] // (2 * PIECES[kind])
         return ref.at[pl.ds(h * (ref.shape[0] // 2) + p * rows, rows)]
 
     w_main = h1 * (u + 2) + (1 - h1) * (u + 1)
@@ -236,26 +243,26 @@
         @pl.when(home)
         def _():
             whole(kind).start()
-            for p in range(PIECES):
+            for p in range(PIECES[kind]):
                 for h in range(2):
                     first(kind, h, p).start()
 
     def launch_main(kind):
-        for p in range(PIECES):
+        for p in range(PIECES[kind]):
             for h in range(2):
                 main(kind, h, p).start()
 
     def launch_extra(kind):
         @pl.when(extra_here)
         def _():
-            for p in range(PIECES):
+            for p in range(PIECES[kind]):
                 for h in range(2):
                     extra(kind, h, p).start()
 
     def serve_z(kind, k):
-        for p in range(PIECES):
+        for p in range(PIECES[kind]):
             z_piece(kind, k, p).wait_recv()
-            if k == 1:
+            if k == 1 and kind == 0:
                 @pl.when(u == 1)
                 def _():
                     passed(kind, p).start()
@@ -263,7 +270,7 @@
             across(kind, 0, k, p, c).start()
 
     def serve_y(kind, k):
-        for p in range(PIECES):
+        for p in range(PIECES[kind]):
             y_in(kind, k, p).wait_recv()
             across(kind, 1, k, p, c).start()
 
@@ -277,7 +284,7 @@
             def _():
                 own_block(kind).wait()
             return
-        for p in range(PIECES):
+        for p in range(PIECES[kind]):
             across(kind, other, k, p, oc).wait_recv()
 
     after = lax.rem(me + 1, n)
@@ -286,7 +293,7 @@
             ref.at[pl.ds(tokens - WINDOW, WINDOW)], ext.at[pl.ds(0, WINDOW)],
             tail_send.at[i], tail_recv.at[i], (after, rank),
         )
-        for i, (ref, ext) in enumerate(((k_ref, key_ext), (v_ref, val_ext)))
+        for i, (ref, ext) in enumerate(((k_hbm, key_ext), (v_hbm, val_ext)))
     ]
     for copy in tails:
         copy.start()
@@ -311,12 +318,10 @@
         own_block(0).start()
         own_block(1).start()
 
-    key_ext[WINDOW:] = k_ref[...]
-    val_ext[WINDOW:] = v_ref[...]
 
     blocks = tokens // WINDOW
     heads_local = q_width // HEAD
-    group = heads_local // (k_ref.shape[1] // HEAD)
+    group = heads_local // (k_hbm.shape[1] // HEAD)
 
     slopes = [
         jnp.exp2(
@@ -386,6 +391,8 @@
             mix_out.at[rows], mix_in.at[rows], mix_send.at[p], mix_recv.at[p], at(ox, y, z, c)
         )
 
+    for copy in loads:
+        copy.wait()
     windows(ox * (blocks // 2) + 1, blocks // 2 - 1)
     for copy in tails:
         copy.wait_recv()
@@ -446,6 +453,10 @@
 
     serve_z(0, 2)
 
+    @pl.when(u == 0)
+    def _():
+        launch_local(1)
+
     @pl.when((u == 0) & away)
     def _():
         launch_main(1)
@@ -459,7 +470,9 @@
     def _():
         launch_main(1)
 
-    launch_local(1)
+    @pl.when(u == 1)
+    def _():
+        launch_local(1)
 
     @pl.when(away)
     def _():
@@ -501,6 +514,11 @@
                 launch_main(1)
 
             serve_z(1, 1)
+
+    @pl.when(u == 1)
+    def _():
+        for p in range(PIECES[1]):
+            passed(1, p).start()
 
     steps = 2 * LAYERS
 
@@ -573,8 +591,10 @@
 
     before = {
         1: [(serve_y, 0)],
-        3: [(serve_z, 2), (serve_y, 1)],
-        5: [(serve_z, 3), (serve_y, 2)],
+        2: [(serve_z, 2)],
+        3: [(serve_y, 1)],
+        4: [(serve_z, 3)],
+        5: [(serve_y, 2)],
         7: [(serve_y, 3)],
     }
     for i in range(steps):
@@ -583,7 +603,10 @@
             serve(1, at_k)
         need(1, other, k)
         downward(i)
-        if i >= 1:
+        if i == 6:
+            for j in range(i):
+                join(j)
+        if i > 6:
             join(i - 1)
     join(steps - 1)
     for k in range(LAYERS):
@@ -604,7 +627,7 @@
         row_copy(1, p).wait_send()
         row_copy(2, p).wait_send()
     for kind in range(2):
-        for p in range(PIECES):
+        for p in range(PIECES[kind]):
             for h in range(2):
                 main(kind, h, p).wait_send()
             for k in range(LAYERS):
@@ -616,21 +639,21 @@
     @pl.when(extra_here)
     def _():
         for kind in range(2):
-            for p in range(PIECES):
+            for p in range(PIECES[kind]):
                 for h in range(2):
                     extra(kind, h, p).wait_send()
 
     @pl.when(u == 1)
     def _():
         for kind in range(2):
-            for p in range(PIECES):
+            for p in range(PIECES[kind]):
                 passed(kind, p).wait_send()
 
     @pl.when(home)
     def _():
         for kind in range(2):
             whole(kind).wait_send()
-            for p in range(PIECES):
+            for p in range(PIECES[kind]):
                 for h in range(2):
                     first(kind, h, p).wait_send()
         for i in range(steps):
@@ -662,9 +685,10 @@
     return pl.pallas_call(
         functools.partial(block_kernel, n, m),
         out_shape=jax.ShapeDtypeStruct(residual.shape, bf16),
-        in_specs=[vmem] * 3 + [smem] + [vmem] * 2 + [pl.BlockSpec(memory_space=pl.ANY)] * 4,
+        in_specs=[smem] + [vmem] * 2 + [pl.BlockSpec(memory_space=pl.ANY)] * 7,
         out_specs=pl.BlockSpec(memory_space=pltpu.VMEM),
         scratch_shapes=[
+            pltpu.VMEM(queries.shape, bf16),
             pltpu.VMEM((tokens + WINDOW, keys.shape[1]), bf16),
             pltpu.VMEM((tokens + WINDOW, keys.shape[1]), bf16),
             pltpu.VMEM(out_weight.shape, bf16),
@@ -693,17 +717,17 @@
             dma((SIDES,)),
             dma((ROW_PARTS,)),
             dma((ROW_PARTS,)),
-            dma((2, 2, PIECES)),
-            dma((2, 2, PIECES)),
-            dma((2, PIECES)),
-            dma((2, LAYERS, PIECES)),
-            dma((2, 2, PIECES)),
-            dma((2, LAYERS, PIECES)),
-            dma((2, LAYERS, PIECES)),
+            dma((2, 2, max(PIECES))),
+            dma((2, 2, max(PIECES))),
+            dma((2, max(PIECES))),
+            dma((2, LAYERS, max(PIECES))),
+            dma((2, 2, max(PIECES))),
+            dma((2, LAYERS, max(PIECES))),
+            dma((2, LAYERS, max(PIECES))),
             dma((2,)),
             dma((2,)),
-            dma((2, 2, LAYERS, PIECES)),
-            dma((2, 2, LAYERS, PIECES)),
+            dma((2, 2, LAYERS, max(PIECES))),
+            dma((2, 2, LAYERS, max(PIECES))),
             dma((3, ROW_PARTS)),
             dma((m, ROW_PARTS)),
             dma((CORES, ROW_PARTS)),
@@ -712,13 +736,13 @@
             dma((steps,)),
             dma((steps, CORES)),
             dma((3, steps)),
-            dma((4,)),
+            dma((7,)),
         ],
         compiler_params=pltpu.CompilerParams(
             collective_id=0, has_side_effects=True, vmem_limit_bytes=60 * 1024 * 1024
         ),
     )(
-        queries, keys, values, sinks, gains, biases, out_weight, up_weight, down_weight, residual,
+        sinks, gains, biases, queries, keys, values, out_weight, up_weight, down_weight, residual,
     )
 
 

time: 135 us -> 130 us (0.963)
  the two profiles are of different devices: /device:TPU:17 before, /device:TPU:1 now
where the time goes in v3:
time: 130 us; the launch traced here: 128 us
  Pallas kernels  126 us (97%)
  local copies, waits for them, and re-layouts  2.09 us (2%)
    pallas_call x1, Pallas kernels, fused_block(): pl.pallas_call(functools.partial(block_kernel, n, m), out_shape=jax.Shape...  126 us

profile of v3, /device:TPU:1, one launch (start us, length us, event | category | flops | bytes accessed | tf_op | source)
XLA Modules:
  0.0 128.1 jit_solution(8161578497606316740)
XLA Ops:
  0.0 126.0 %shard_map.100 = bf16[192,2048]{1,0:T(8,128)(2,1)} custom-call(f32[3]{0:T(128)} %sinks_ref.1, f32[2,2048]{1,0:T(2,128)} %gains_ref.1, f32[2,2048]{1,0:T(2,128)} %biases_ref.1, bf16[768,384]{1,0:T(8,128)(2,1)} %q_hbm.1, bf16[768,128]{1,0:T(8,128)(2,1)} %k_hbm.1, bf16[768,128]{1,0:T(8,128)(2,1)} %v_hbm.1, bf16[384,2048]{1,0:T(8,128)(2,1)} %proj_hbm.1, ...), custom_call_target="tpu_custom_call" | custom-call | tf_op jit(solution)/shard_map/pallas_call | solution.py:685
  126.0 2.1 %copy.12 = bf16[192,2048]{1,0:T(8,128)(2,1)} copy(bf16[192,2048]{1,0:T(8,128)(2,1)} %shard_map.100) | data formatting | bytes 1572864

commit v4 on v3

--- a/solution.py
+++ b/solution.py
@@ -295,8 +295,11 @@
         )
         for i, (ref, ext) in enumerate(((k_hbm, key_ext), (v_hbm, val_ext)))
     ]
-    for copy in tails:
-        copy.start()
+    @pl.when(me != n - 1)
+    def _():
+        for copy in tails:
+            copy.start()
+
     launch_main(0)
     launch_extra(0)
     proj_copy = remote(proj_hbm, proj_in, proj_send.at[0], proj_recv.at[0], at(x, y, z, oc))
@@ -394,8 +397,16 @@
     for copy in loads:
         copy.wait()
     windows(ox * (blocks // 2) + 1, blocks // 2 - 1)
-    for copy in tails:
-        copy.wait_recv()
+    @pl.when(me != 0)
+    def _():
+        for copy in tails:
+            copy.wait_recv()
+
+    @pl.when(me == 0)
+    def _():
+        key_ext[:WINDOW] = jnp.zeros_like(key_ext[:WINDOW])
+        val_ext[:WINDOW] = jnp.zeros_like(val_ext[:WINDOW])
+
     windows(ox * (blocks // 2), 1)
     swap(0, ox).start()
     proj_local.wait()
@@ -547,9 +558,12 @@
 
     def downward(i):
         s = column(i // 2, i % 2)
-        terms[i] = jnp.dot(
-            act[...], down_all[s], preferred_element_type=jnp.float32
-        ).astype(jnp.bfloat16)
+        @pl.loop(0, 2)
+        def _(r):
+            rows = pl.ds(pl.multiple_of(r * (tokens // 2), tokens // 2), tokens // 2)
+            terms[i, rows] = jnp.dot(
+                act[rows], down_all[s], preferred_element_type=jnp.float32
+            ).astype(jnp.bfloat16)
 
         @pl.when(home)
         def _():
@@ -617,8 +631,11 @@
         rows = pl.ds(pl.multiple_of(i * step_rows, step_rows), step_rows)
         out_ref[rows] = norm_rows(total[rows], gains_ref[1:2], biases_ref[1:2]).astype(jnp.bfloat16)
 
-    for copy in tails:
-        copy.wait_send()
+    @pl.when(me != n - 1)
+    def _():
+        for copy in tails:
+            copy.wait_send()
+
     proj_copy.wait_send()
     swap(0, ox).wait_send()
     swap(1, x).wait_send()

time: 130 us -> 129 us (level)
  no operation moved by 1% of the time
where the time goes in v4:
time: 129 us; the launch traced here: 127 us
  Pallas kernels  125 us (97%)
  local copies, waits for them, and re-layouts  2.09 us (2%)
    pallas_call x1, Pallas kernels, fused_block(): pl.pallas_call(functools.partial(block_kernel, n, m), out_shape=jax.Shape...  125 us

profile of v4, /device:TPU:1, one launch (start us, length us, event | category | flops | bytes accessed | tf_op | source)
XLA Modules:
  0.0 126.9 jit_solution(1176023514146014372)
XLA Ops:
  0.0 124.8 %shard_map.100 = bf16[192,2048]{1,0:T(8,128)(2,1)} custom-call(f32[3]{0:T(128)} %sinks_ref.1, f32[2,2048]{1,0:T(2,128)} %gains_ref.1, f32[2,2048]{1,0:T(2,128)} %biases_ref.1, bf16[768,384]{1,0:T(8,128)(2,1)} %q_hbm.1, bf16[768,128]{1,0:T(8,128)(2,1)} %k_hbm.1, bf16[768,128]{1,0:T(8,128)(2,1)} %v_hbm.1, bf16[384,2048]{1,0:T(8,128)(2,1)} %proj_hbm.1, ...), custom_call_target="tpu_custom_call" | custom-call | tf_op jit(solution)/shard_map/pallas_call | solution.py:702
  124.8 2.1 %copy.12 = bf16[192,2048]{1,0:T(8,128)(2,1)} copy(bf16[192,2048]{1,0:T(8,128)(2,1)} %shard_map.100) | data formatting | bytes 1572864
